TPU v7x, 32 devices: a whole 2x2x4 slice. The times are simulated.
32 devices in a mesh: fs: 16 (over z, y, x), tp: 2 (over core).
Axes of the slice: x: 2, y: 2, z: 4, core: 2. Of those that a mesh axis runs over, the one named last changes fastest.
Arguments:
- normed: bfloat16 [16384, 2048], P('fs'), may hold values from -6 to 6
- key_cot: bfloat16 [16384, 1024], P('fs', 'tp'), may hold values from -130 to 130
- value_cot: bfloat16 [16384, 2048], P('fs', 'tp'), may hold values from -130 to 130
- basis: bfloat16 [2048, 256], P('fs'), may hold values from -3.535534 to 3.535534
- master_key: float32 [2048, 1024], P('fs', 'tp'), may hold values from -3 to 3
- master_value: float32 [2048, 2048], P('fs', 'tp'), may hold values from -3 to 3
- first_key: float32 [256, 1024], P('fs', 'tp'), may hold values from -3 to 3
- second_key: float32 [256, 1024], P('fs', 'tp'), may hold values from 0.05 to 2
- first_value: float32 [256, 2048], P('fs', 'tp'), may hold values from -3 to 3
- second_value: float32 [256, 2048], P('fs', 'tp'), may hold values from 0.05 to 2
Outputs:
- step_key: float32 [2048, 1024], P('fs', 'tp')
- step_value: float32 [2048, 2048], P('fs', 'tp')
- new_master_key: float32 [2048, 1024], P('fs', 'tp')
- new_master_value: float32 [2048, 2048], P('fs', 'tp')
- copy_key: bfloat16 [2048, 1024], P(None, 'tp')
- copy_value: bfloat16 [2048, 2048], P(None, 'tp')
- new_first_key: float32 [256, 1024], P('fs', 'tp')
- new_second_key: float32 [256, 1024], P('fs', 'tp')
- new_first_value: float32 [256, 2048], P('fs', 'tp')
- new_second_value: float32 [256, 2048], P('fs', 'tp')
All inputs are finite; a program needn't handle non-finite values.
Results may differ from a plain program's by a relative error of at most 0.0055.
Values may be sent and summed in bfloat16 or wider, within the bound.
A program may use at most 64 MiB of HBM per device.

v0:
```python
import jax
import jax.numpy as jnp
from jax import lax
from jax.sharding import PartitionSpec as P

DK = 1024
DV = 2048
R = 256
learn_rate = 0.05
beta_first = 0.9
beta_second = 0.9
epsilon = 1e-08
norm_eps = 1e-06


def on_device(
    normed,
    key_cot,
    value_cot,
    basis,
    master_key,
    master_value,
    first_key,
    second_key,
    first_value,
    second_value,
):
    key_cols = key_cot.shape[1]
    cotangents = jnp.concatenate([key_cot, value_cot], axis=1)
    projected = jnp.dot(
        normed, lax.all_gather(basis, "fs", axis=0, tiled=True), preferred_element_type=jnp.float32
    )
    upper_part = projected.astype(jnp.bfloat16)
    lower_part = (projected - upper_part.astype(jnp.float32)).astype(jnp.bfloat16)
    partial_value = lax.dot_general(
        upper_part, cotangents, (((0,), (0,)), ((), ())), preferred_element_type=jnp.float32
    )
    partial_value = partial_value + lax.dot_general(
        lower_part, cotangents, (((0,), (0,)), ((), ())), preferred_element_type=jnp.float32
    )
    rank_rows = first_key.shape[0]
    summed = lax.psum(partial_value, "fs")
    squares = lax.psum(jnp.sum(summed * summed), "tp")
    own_rows = lax.dynamic_slice_in_dim(summed, lax.axis_index("fs") * rank_rows, rank_rows, 0)
    root_mean = jnp.sqrt(squares / (R * (DK + DV)) + norm_eps)
    grad_scale = 1.0 / root_mean
    first_moment = jnp.concatenate([first_key, first_value], axis=1)
    second_moment = jnp.concatenate([second_key, second_value], axis=1)
    scaled = own_rows * grad_scale
    new_first = beta_first * first_moment + (1.0 - beta_first) * scaled
    new_second = beta_second * second_moment + (1.0 - beta_second) * scaled * scaled
    direction = (new_first / (jnp.sqrt(new_second) + epsilon)).astype(jnp.bfloat16)
    all_directions = lax.all_gather(direction, "fs", axis=0, tiled=True)
    update_step = jnp.dot(basis, all_directions, preferred_element_type=jnp.float32)
    master = jnp.concatenate([master_key, master_value], axis=1)
    new_master = master - learn_rate * update_step
    half_copy = new_master.astype(jnp.bfloat16)
    copy_key, copy_value = (
        lax.all_gather(half_copy[:, :key_cols], "fs", axis=0, tiled=True),
        lax.all_gather(half_copy[:, key_cols:], "fs", axis=0, tiled=True),
    )
    return (
        update_step[:, :key_cols],
        update_step[:, key_cols:],
        new_master[:, :key_cols],
        new_master[:, key_cols:],
        copy_key,
        copy_value,
        new_first[:, :key_cols],
        new_second[:, :key_cols],
        new_first[:, key_cols:],
        new_second[:, key_cols:],
    )


def solution(mesh):
    placed = (
        P("fs", None),
        P("fs", "tp"),
        P("fs", "tp"),
        P("fs", None),
        P("fs", "tp"),
        P("fs", "tp"),
        P("fs", "tp"),
        P("fs", "tp"),
        P("fs", "tp"),
        P("fs", "tp"),
    )
    return jax.shard_map(
        on_device,
        mesh=mesh,
        in_specs=placed,
        out_specs=(
            P("fs", "tp"),
            P("fs", "tp"),
            P("fs", "tp"),
            P("fs", "tp"),
            P(None, "tp"),
            P(None, "tp"),
            P("fs", "tp"),
            P("fs", "tp"),
            P("fs", "tp"),
            P("fs", "tp"),
        ),
        check_vma=False,
    )
```

profile of v0, /device:TPU:0, one launch (start us, length us, event | category | flops | bytes accessed | tf_op | source)
XLA Modules:
  0.0 406.0 jit_solution(744935510458757411)
XLA Ops:
  7.2 0.0 all-gather.4.cloned.1.call-start
  7.2 0.7 all-gather.4.cloned.1.call-update
  7.9 0.0 all-reduce.2.cloned.1.call-start
  8.0 0.0 copy-start
  8.0 1.4 constant_dynamic-update-slice_fusion.1
  9.4 0.5 copy-done
  9.9 0.2 constant_dynamic-update-slice_fusion
  10.0 58.5 %all-gather.4.cloned.1.call-done = bf16[2048,256]{1,0:T(8,128)(2,1)} async-done(((bf16[128,256]{1,0:T(8,128)(2,1)}), bf16[2048,256]{1,0:T(8,128)(2,1)}) %all-gather.4.cloned.1.call-update) | async-done | bytes 1048592 | tf_op jit(solution)/shard_map/all_gather | solution.py:31
  68.6 3.7 fusion.6
  72.3 1.0 fusion.1
  73.4 0.0 copy-start.2
  73.4 2.2 convolution_add_fusion
  75.5 0.0 copy-start.3
  75.5 0.0 copy-start.4
  75.5 0.0 copy-start.1
  75.6 0.0 all-reduce.2.cloned.1.call-update
  75.6 0.0 all-gather.6.cloned.1.call-start
  75.6 0.0 copy-done.2
  75.7 0.1 copy.20
  75.8 1.2 copy.21
  77.0 115.1 %all-reduce.2.cloned.1.call-done = f32[256,1536]{1,0:T(8,128)} async-done(((f32[256,1536]{1,0:T(8,128)}), f32[256,1536]{1,0:T(8,128)}) %all-reduce.2.cloned.1.call-update) | async-done | bytes 1572880 | tf_op jit(solution)/shard_map/psum | solution.py:42
  192.1 2.4 multiply_reduce_fusion
  194.5 3.1 psum.15
  198.3 0.0 copy-done.3
  198.3 0.0 copy-done.4
  198.3 0.0 copy-done.5
  198.3 0.0 copy-done.6
  198.3 1.0 divide_convert_fusion
  199.3 43.7 %all_gather.13 = bf16[256,1536]{1,0:T(8,128)(2,1)S(1)} all-gather(bf16[16,1536]{1,0:T(8,128)(2,1)S(1)} %get-tuple-element.22), channel_id=1, replica_groups=mesh['fs'=16,'tp'=2] {'fs'}, dimensions={0}, use_global_device_ids=true | all-gather | bytes 835584 | tf_op jit(solution)/shard_map/all_gather | solution.py:53
  243.0 0.0 copy-done.1
  243.0 0.4 fusion.4
  243.4 0.7 slice.44
  244.1 0.0 all-gather.6.cloned.1.call-update
  244.1 0.0 all-gather.8.cloned.1.call-start
  244.1 0.7 slice.45
  244.9 0.0 all-gather.8.cloned.1.call-update
  244.9 0.6 slice.47
  245.5 0.6 slice.49
  246.1 0.6 slice.46
  246.7 0.6 slice.48
  247.5 1.0 copy.25
  248.5 0.8 copy.24
  249.4 1.0 copy.23
  250.3 0.8 copy.22
  251.2 51.9 %all-gather.6.cloned.1.call-done = bf16[2048,512]{0,1:T(8,128)(2,1)} async-done(((bf16[128,512]{0,1:T(8,128)(2,1)}), bf16[2048,512]{0,1:T(8,128)(2,1)}) %all-gather.6.cloned.1.call-update) | async-done | bytes 2097168 | tf_op jit(solution)/shard_map/all_gather | solution.py:59
  303.0 3.9 copy.26
  307.0 86.1 %all-gather.8.cloned.1.call-done = bf16[2048,1024]{0,1:T(8,128)(2,1)} async-done(((bf16[128,1024]{0,1:T(8,128)(2,1)}), bf16[2048,1024]{0,1:T(8,128)(2,1)}) %all-gather.8.cloned.1.call-update) | async-done | bytes 4194320 | tf_op jit(solution)/shard_map/all_gather | solution.py:60
  393.1 6.4 %copy.27 = bf16[2048,1024]{1,0:T(8,128)(2,1)} copy(bf16[2048,1024]{0,1:T(8,128)(2,1)} %all-gather.8.cloned.1.call-done) | data formatting | bytes 8388608
  (6 shorter events, 0.1 us)
Async XLA Ops:
  7.2 61.4 %all-gather.4.cloned.1.call-start = ((), (), s32[]{:S(2)}) async-start(), calls=%async_computation | async-start | bytes 1114112 | tf_op jit(solution)/shard_map/all_gather | solution.py:31
  7.9 184.2 %all-reduce.2.cloned.1.call-start = ((), (), s32[]{:S(2)}) async-start(), calls=%async_computation.1 | async-start | bytes 3145728 | tf_op jit(solution)/shard_map/psum | solution.py:42
  8.0 1.9 copy-start
  73.4 2.3 copy-start.2
  75.5 122.7 %copy-start.3 = (f32[16,1024]{1,0:T(8,128)S(1)}, f32[16,1024]{1,0:T(8,128)}, u32[]{:S(2)}) copy-start(f32[16,1024]{1,0:T(8,128)} %param.19) | copy-start | bytes 196612
  75.5 122.8 %copy-start.4 = (f32[16,1024]{1,0:T(8,128)S(1)}, f32[16,1024]{1,0:T(8,128)}, u32[]{:S(2)}) copy-start(f32[16,1024]{1,0:T(8,128)} %param.18) | copy-start | bytes 196612
  75.5 122.8 %copy-start.5 = (f32[16,512]{1,0:T(8,128)S(1)}, f32[16,512]{1,0:T(8,128)}, u32[]{:S(2)}) copy-start(f32[16,512]{1,0:T(8,128)} %param.17) | copy-start | bytes 98308
  75.5 122.8 %copy-start.6 = (f32[16,512]{1,0:T(8,128)S(1)}, f32[16,512]{1,0:T(8,128)}, u32[]{:S(2)}) copy-start(f32[16,512]{1,0:T(8,128)} %param.16) | copy-start | bytes 98308
  75.5 167.4 %copy-start.1 = (bf16[128,256]{1,0:T(8,128)(2,1)S(1)}, bf16[128,256]{1,0:T(8,128)(2,1)}, u32[]{:S(2)}) copy-start(bf16[128,256]{1,0:T(8,128)(2,1)} %param.13) | copy-start | bytes 196612
  75.6 227.5 %all-gather.6.cloned.1.call-start = ((), (), s32[]{:S(2)}) async-start(), calls=%async_computation.2 | async-start | bytes 2228224 | tf_op jit(solution)/shard_map/all_gather | solution.py:59
  244.1 149.0 %all-gather.8.cloned.1.call-start = ((), (), s32[]{:S(2)}) async-start(), calls=%async_computation.3 | async-start | bytes 4456448 | tf_op jit(solution)/shard_map/all_gather | solution.py:60
Sparse Core Ops, SparseCore 0:
  10.7 57.7 all-gather.3
  75.7 116.3 all-reduce.1
  244.2 58.7 all-gather.5
  306.2 86.8 all-gather.7
where the time goes:
time: 406 us
  waiting for transfers between devices  312 us (77%)
  blocking collectives  46.8 us (12%)
  local copies, waits for them, and re-layouts  21.4 us (5%)
  between operations  14.6 us (4%)
  matrix products  7.34 us (2%)
    psum x1, waiting for transfers between devices, on_device(): summed = lax.psum(partial_value, 'fs')  115 us
    all_gather x1, waiting for transfers between devices, on_device(): lax.all_gather(half_copy[:, key_cols:], 'fs', axis=0, tiled=True)  86.1 us
    all_gather x1, waiting for transfers between devices, on_device(): lax.all_gather(basis, 'fs', axis=0, tiled=True)  58.5 us
    all_gather x1, waiting for transfers between devices, on_device(): lax.all_gather(half_copy[:, :key_cols], 'fs', axis=0, tiled=True)  51.9 us
    all_gather x1, blocking collectives, on_device(): all_directions = lax.all_gather(direction, 'fs', axis=0, tiled=True)  43.7 us
    unnamed x23, local copies, waits for them, and re-layouts  17.3 us
  transfers between devices with their start and end apart: 4, of which 4 were waited for; matrix products, arithmetic and copies ran while one was open for 3% of the time, Pallas kernels for 0%

commit v1 on v0

--- a/solution.py
+++ b/solution.py
@@ -11,6 +11,15 @@
 beta_second = 0.9
 epsilon = 1e-08
 norm_eps = 1e-06
+
+
+def sum_by_hops(x, axis):
+    size = lax.axis_size(axis)
+    acc, hop = (x, 1)
+    while hop < size:
+        acc = acc + lax.ppermute(acc, axis, [(i, i ^ hop) for i in range(size)])
+        hop = 2 * hop
+    return acc
 
 
 def on_device(
@@ -39,7 +48,7 @@
         lower_part, cotangents, (((0,), (0,)), ((), ())), preferred_element_type=jnp.float32
     )
     rank_rows = first_key.shape[0]
-    summed = lax.psum(partial_value, "fs")
+    summed = sum_by_hops(partial_value, "fs")
     squares = lax.psum(jnp.sum(summed * summed), "tp")
     own_rows = lax.dynamic_slice_in_dim(summed, lax.axis_index("fs") * rank_rows, rank_rows, 0)
     root_mean = jnp.sqrt(squares / (R * (DK + DV)) + norm_eps)

time: 406 us -> 456 us (1.12)
  waiting for transfers between devices: 312 us -> 357 us
  starting transfers between devices: 0.16 us -> 6.29 us
    ppermute x0 -> x4, waiting for transfers between devices: none -> 160 us  [sum_by_hops(): acc = acc + lax.ppermute(acc, axis, [(i, i ^ hop) for i in range(size)])]
    psum x1 -> x0, waiting for transfers between devices: 115 us -> none  [on_device(): summed = lax.psum(partial_value, 'fs')]
    ppermute x0 -> x4, starting transfers between devices: none -> 6.17 us  [sum_by_hops(): acc = acc + lax.ppermute(acc, axis, [(i, i ^ hop) for i in range(size)])]
    unnamed x23 -> x25, local copies, waits for them, and re-layouts: 17.3 us -> 16.2 us
  transfers between devices with their start and end apart: 4 -> 7, of which waited for: 4 -> 7; matrix products, arithmetic and copies ran while one was open for 3% -> 3% of each run, Pallas kernels for 0% -> 0%
where the time goes in v1:
time: 456 us
  waiting for transfers between devices  357 us (78%)
  blocking collectives  46 us (10%)
  local copies, waits for them, and re-layouts  20.4 us (4%)
  between operations  14.6 us (3%)
  starting transfers between devices  6.29 us (1%)
  matrix products  6.2 us (1%)
  other arithmetic  5.04 us (1%)
    ppermute x4, waiting for transfers between devices, sum_by_hops(): acc = acc + lax.ppermute(acc, axis, [(i, i ^ hop) for i in range(size)])  160 us
    all_gather x1, waiting for transfers between devices, on_device(): lax.all_gather(half_copy[:, key_cols:], 'fs', axis=0, tiled=True)  86.3 us
    all_gather x1, waiting for transfers between devices, on_device(): lax.all_gather(basis, 'fs', axis=0, tiled=True)  58.5 us
    all_gather x1, waiting for transfers between devices, on_device(): lax.all_gather(half_copy[:, :key_cols], 'fs', axis=0, tiled=True)  51.9 us
    all_gather x1, blocking collectives, on_device(): all_directions = lax.all_gather(direction, 'fs', axis=0, tiled=True)  42.9 us
    unnamed x25, local copies, waits for them, and re-layouts  16.2 us
  transfers between devices with their start and end apart: 7, of which 7 were waited for; matrix products, arithmetic and copies ran while one was open for 3% of the time, Pallas kernels for 0%

profile of v1, /device:TPU:0, one launch (start us, length us, event | category | flops | bytes accessed | tf_op | source)
XLA Modules:
  0.0 455.9 jit_solution(574507813580780460)
XLA Ops:
  7.2 0.0 all-gather.4.cloned.1.call-start
  7.2 0.7 all-gather.4.cloned.1.call-update
  7.9 0.0 all-gather.6.cloned.1.call-start
  8.0 1.4 constant_dynamic-update-slice_fusion.1
  9.4 0.5 copy-done
  9.9 0.2 constant_dynamic-update-slice_fusion
  10.0 58.5 %all-gather.4.cloned.1.call-done = bf16[2048,256]{1,0:T(8,128)(2,1)} async-done(((bf16[128,256]{1,0:T(8,128)(2,1)}), bf16[2048,256]{1,0:T(8,128)(2,1)}) %all-gather.4.cloned.1.call-update) | async-done | bytes 1048592 | tf_op jit(solution)/shard_map/all_gather | solution.py:40
  68.6 3.7 fusion.6
  72.3 1.0 fusion.1
  73.4 1.0 convolution_add_fusion
  74.4 1.5 collective-permute-start
  75.9 32.7 %collective-permute-done = f32[256,1536]{1,0:T(8,128)S(1)} collective-permute-done((f32[256,1536]{1,0:T(8,128)S(1)}, f32[256,1536]{1,0:T(8,128)S(1)}, u32[]{:S(2)}, u32[]{:S(2)}) %collective-permute-start) | collective-permute-done | bytes 1572896 | tf_op jit(solution)/shard_map/ppermute | solution.py:20
  108.6 0.2 add.36
  108.8 1.5 collective-permute-start.1
  110.4 31.9 %collective-permute-done.1 = f32[256,1536]{1,0:T(8,128)S(1)} collective-permute-done((f32[256,1536]{1,0:T(8,128)S(1)}, f32[256,1536]{1,0:T(8,128)S(1)}, u32[]{:S(2)}, u32[]{:S(2)}) %collective-permute-start.1) | collective-permute-done | bytes 1572896 | tf_op jit(solution)/shard_map/ppermute | solution.py:20
  142.2 0.2 add.37
  142.4 0.0 copy-start.3
  142.4 0.0 copy-start.1
  142.4 1.0 collective-permute-start.2
  143.4 33.2 %collective-permute-done.2 = f32[256,1536]{1,0:T(8,128)S(1)} collective-permute-done((f32[256,1536]{1,0:T(8,128)S(1)}, f32[256,1536]{1,0:T(8,128)S(1)}, u32[]{:S(2)}, u32[]{:S(2)}) %collective-permute-start.2) | collective-permute-done | bytes 1572896 | tf_op jit(solution)/shard_map/ppermute | solution.py:20
  176.6 0.2 add.38
  176.8 2.2 collective-permute-start.3
  179.0 0.1 copy.20
  179.1 0.2 copy.21
  179.3 0.0 copy-start.6
  179.4 62.2 %collective-permute-done.3 = f32[256,1536]{1,0:T(8,128)} collective-permute-done((f32[256,1536]{1,0:T(8,128)S(1)}, f32[256,1536]{1,0:T(8,128)}, u32[]{:S(2)}, u32[]{:S(2)}) %collective-permute-start.3) | collective-permute-done | bytes 1572896 | tf_op jit(solution)/shard_map/ppermute | solution.py:20
  241.5 3.5 multiply_reduce_fusion
  245.0 3.1 psum.7
  248.9 1.0 divide_convert_fusion
  249.8 42.9 %all_gather.13 = bf16[256,1536]{1,0:T(8,128)(2,1)S(1)} all-gather(bf16[16,1536]{1,0:T(8,128)(2,1)S(1)} %get-tuple-element.22), channel_id=1, replica_groups=mesh['fs'=16,'tp'=2] {'fs'}, dimensions={0}, use_global_device_ids=true | all-gather | bytes 835584 | tf_op jit(solution)/shard_map/all_gather | solution.py:62
  292.7 0.4 fusion.4
  293.1 0.7 slice.44
  293.8 0.0 all-gather.6.cloned.1.call-update
  293.8 0.0 all-gather.8.cloned.1.call-start
  293.9 0.7 slice.45
  294.6 0.0 all-gather.8.cloned.1.call-update
  294.6 0.6 slice.47
  295.2 0.6 slice.49
  295.9 0.6 slice.46
  296.5 0.6 slice.48
  297.3 1.0 copy.25
  298.3 0.8 copy.24
  299.1 1.0 copy.23
  300.1 0.8 copy.22
  300.9 51.9 %all-gather.6.cloned.1.call-done = bf16[2048,512]{0,1:T(8,128)(2,1)} async-done(((bf16[128,512]{0,1:T(8,128)(2,1)}), bf16[2048,512]{0,1:T(8,128)(2,1)}) %all-gather.6.cloned.1.call-update) | async-done | bytes 2097168 | tf_op jit(solution)/shard_map/all_gather | solution.py:68
  352.8 3.9 copy.26
  356.7 86.3 %all-gather.8.cloned.1.call-done = bf16[2048,1024]{0,1:T(8,128)(2,1)} async-done(((bf16[128,1024]{0,1:T(8,128)(2,1)}), bf16[2048,1024]{0,1:T(8,128)(2,1)}) %all-gather.8.cloned.1.call-update) | async-done | bytes 4194320 | tf_op jit(solution)/shard_map/all_gather | solution.py:69
  443.0 6.4 %copy.27 = bf16[2048,1024]{1,0:T(8,128)(2,1)} copy(bf16[2048,1024]{0,1:T(8,128)(2,1)} %all-gather.8.cloned.1.call-done) | data formatting | bytes 8388608
  (16 shorter events, 0.1 us)
Async XLA Ops:
  7.2 61.4 %all-gather.4.cloned.1.call-start = ((), (), s32[]{:S(2)}) async-start(), calls=%async_computation | async-start | bytes 1114112 | tf_op jit(solution)/shard_map/all_gather | solution.py:40
  7.9 344.9 %all-gather.6.cloned.1.call-start = ((), (), s32[]{:S(2)}) async-start(), calls=%async_computation.1 | async-start | bytes 2228224 | tf_op jit(solution)/shard_map/all_gather | solution.py:68
  8.0 1.9 copy-start
  74.4 34.2 %collective-permute-start = (f32[256,1536]{1,0:T(8,128)S(1)}, f32[256,1536]{1,0:T(8,128)S(1)}, u32[]{:S(2)}, u32[]{:S(2)}) collective-permute-start(f32[256,1536]{1,0:T(8,128)S(1)} %convolution_add_fusion), channel_id=1, source_target_pairs={{0,2},{2,0},{4,6},{6,4},{8,10},{10,8},{12,14},{14,12},{16,18},{18,... | collective-permute-start | bytes 4718600 | tf_op jit(solution)/shard_map/ppermute | solution.py:20
  108.8 33.4 %collective-permute-start.1 = (f32[256,1536]{1,0:T(8,128)S(1)}, f32[256,1536]{1,0:T(8,128)S(1)}, u32[]{:S(2)}, u32[]{:S(2)}) collective-permute-start(f32[256,1536]{1,0:T(8,128)S(1)} %add.36), channel_id=1, source_target_pairs={{0,4},{2,6},{4,0},{6,2},{8,12},{10,14},{12,8},{14,10},{16,20},{18,... | collective-permute-start | bytes 4718600 | tf_op jit(solution)/shard_map/ppermute | solution.py:20
  142.4 36.6 %copy-start.3 = (f32[128,512]{1,0:T(8,128)S(1)}, f32[128,512]{1,0:T(8,128)}, u32[]{:S(2)}) copy-start(f32[128,512]{1,0:T(8,128)} %param.14) | copy-start | bytes 786436
  142.4 36.7 %copy-start.1 = (f32[128,1024]{1,0:T(8,128)S(1)}, f32[128,1024]{1,0:T(8,128)}, u32[]{:S(2)}) copy-start(f32[128,1024]{1,0:T(8,128)} %param.15) | copy-start | bytes 1572868
  142.4 34.2 %collective-permute-start.2 = (f32[256,1536]{1,0:T(8,128)S(1)}, f32[256,1536]{1,0:T(8,128)S(1)}, u32[]{:S(2)}, u32[]{:S(2)}) collective-permute-start(f32[256,1536]{1,0:T(8,128)S(1)} %add.37), channel_id=1, source_target_pairs={{0,8},{2,10},{4,12},{6,14},{8,0},{10,2},{12,4},{14,6},{16,24},{18,... | collective-permute-start | bytes 4718600 | tf_op jit(solution)/shard_map/ppermute | solution.py:20
  176.8 64.7 %collective-permute-start.3 = (f32[256,1536]{1,0:T(8,128)S(1)}, f32[256,1536]{1,0:T(8,128)}, u32[]{:S(2)}, u32[]{:S(2)}) collective-permute-start(f32[256,1536]{1,0:T(8,128)S(1)} %add.38), channel_id=1, source_target_pairs={{0,16},{2,18},{4,20},{6,22},{8,24},{10,26},{12,28},{14,30},{16,0},... | collective-permute-start | bytes 4718600 | tf_op jit(solution)/shard_map/ppermute | solution.py:20
  179.3 69.5 %copy-start.4 = (f32[16,1024]{1,0:T(8,128)S(1)}, f32[16,1024]{1,0:T(8,128)}, u32[]{:S(2)}) copy-start(f32[16,1024]{1,0:T(8,128)} %param.19) | copy-start | bytes 196612
  179.3 69.5 %copy-start.5 = (f32[16,1024]{1,0:T(8,128)S(1)}, f32[16,1024]{1,0:T(8,128)}, u32[]{:S(2)}) copy-start(f32[16,1024]{1,0:T(8,128)} %param.18) | copy-start | bytes 196612
  179.3 69.5 %copy-start.6 = (f32[16,512]{1,0:T(8,128)S(1)}, f32[16,512]{1,0:T(8,128)}, u32[]{:S(2)}) copy-start(f32[16,512]{1,0:T(8,128)} %param.17) | copy-start | bytes 98308
  179.3 69.5 %copy-start.7 = (f32[16,512]{1,0:T(8,128)S(1)}, f32[16,512]{1,0:T(8,128)}, u32[]{:S(2)}) copy-start(f32[16,512]{1,0:T(8,128)} %param.16) | copy-start | bytes 98308
  179.4 113.4 %copy-start.2 = (bf16[128,256]{1,0:T(8,128)(2,1)S(1)}, bf16[128,256]{1,0:T(8,128)(2,1)}, u32[]{:S(2)}) copy-start(bf16[128,256]{1,0:T(8,128)(2,1)} %param.13) | copy-start | bytes 196612
  293.8 149.2 %all-gather.8.cloned.1.call-start = ((), (), s32[]{:S(2)}) async-start(), calls=%async_computation.2 | async-start | bytes 4456448 | tf_op jit(solution)/shard_map/all_gather | solution.py:69
Sparse Core Ops, SparseCore 0:
  10.7 57.7 all-gather.3
  294.0 58.7 all-gather.5
  356.1 86.8 all-gather.7
